TPU v7x, 32 devices: a whole 2x2x4 slice. The times are simulated.
32 devices in a mesh: sp: 8 (over z, y), tp: 4 (over x, core).
Axes of the slice: x: 2, y: 2, z: 4, core: 2. Of those that a mesh axis runs over, the one named last changes fastest.
Arguments:
- tokens: bfloat16 [3072, 2048], P('sp'), may hold values from -6 to 6
- in_gain: float32 [2048], replicated, may hold values from 0.1 to 1.9
- query_weight: bfloat16 [2048, 1024], P(None, 'tp'), may hold values from -0.125 to 0.125
- key_weight: bfloat16 [2048, 1024], P(None, 'tp'), may hold values from -0.125 to 0.125
- value_weight: bfloat16 [2048, 2048], P(None, 'tp'), may hold values from -0.125 to 0.125
- gate_weight: bfloat16 [2048, 2048], P(None, 'tp'), may hold values from -0.125 to 0.125
- decay_down: bfloat16 [2048, 32], replicated, may hold values from -0.125 to 0.125
- decay_up: bfloat16 [32, 1024], replicated, may hold values from -1 to 1
- decay_offset: float32 [1024], P('tp')
- decay_extra: float32 [3072, 1024], P('sp', 'tp'), may hold values from -2 to 0, as said below
- head_gain: float32 [2048], P('tp'), may hold values from 0.1 to 1.9
- out_weight: bfloat16 [2048, 2048], P(None, 'tp'), may hold values from -4 to 4
- out_gain: float32 [2048], P('tp'), may hold values from 0.1 to 1.9
Outputs:
- layer_output: bfloat16 [3072, 2048], P('sp', 'tp')
Inputs may be any that keep to these rules, and one draw needn't show every extreme that they name: `decay_extra`: never positive.
All inputs are finite; a program needn't handle non-finite values.
Results may differ from a plain program's by a relative error of at most 0.015.
Values may be sent and summed in bfloat16 or wider, within the bound.
A program may use at most 64 MiB of HBM per device.

v0:
```python
import functools

import jax
import jax.numpy as jnp
from jax import lax
from jax.experimental import pallas as pl
from jax.experimental.pallas import tpu as pltpu
from jax.sharding import PartitionSpec as P

QF = 128
DV = 256
BLK = 128
HALF = 64
EPS = 1e-06
F32 = jnp.float32
BF16 = jnp.bfloat16
MESH = pl.DeviceIdType.MESH


def loop(count, body, carry):
    if count <= 16:
        for i in range(count):
            carry = body(i, carry)
        return carry
    return lax.fori_loop(0, count, body, carry)


def split3(x):
    hi = x.astype(BF16)
    rest = x - hi.astype(F32)
    mid = rest.astype(BF16)
    lo = (rest - mid.astype(F32)).astype(BF16)
    return hi, mid, lo


def dot(a, b):
    return jnp.dot(a, b, preferred_element_type=F32)


def dot_nt(a, b):
    return lax.dot_general(a, b, (((1,), (1,)), ((), ())), preferred_element_type=F32)


def dot_tn(a, b):
    return lax.dot_general(a, b, (((0,), (0,)), ((), ())), preferred_element_type=F32)


def kernel(
    n, n_tp, owners, piece, start,
    tok_hbm, in_gain_hbm, wq_hbm, wk_hbm, wv_hbm, wg_hbm, down_hbm, up_hbm, offset_hbm,
    extra_hbm, head_gain_hbm, wo_hbm,
    mix,
    tok, wq, wk, wv, wg, down, up, extra, wo, in_gain, offset, head_gain,
    nrm, q_s, k_s, v_s, g_s, cum_s, att, qd_s, before,
    send1, recv1, send2, recv2, gath, sq,
    load_sem, s1_sem, r1_sem, s2_sem, r2_sem, gs_sem, gr_sem, qs_sem, qr_sem,
):
    rows, width = tok.shape
    chans = wk.shape[1]
    heads = chans // QF
    vals = wv.shape[1]
    blocks = rows // BLK
    me = lax.axis_index("sp")
    tp = lax.axis_index("tp")
    chips = n_tp // 2
    core = lax.rem(tp, 2)
    chip = tp // 2
    partner = chip * 2 + (1 - core)
    own = me - start
    owning = jnp.logical_and(own >= 0, own < owners)

    first = pl.multiple_of(tp * chans, chans)
    loads = [
        pltpu.make_async_copy(src, dst, load_sem.at[i])
        for i, (src, dst) in enumerate(
            (
                (tok_hbm, tok),
                (wk_hbm, wk),
                (down_hbm, down),
                (up_hbm.at[:, pl.ds(first, chans)], up),
                (extra_hbm, extra),
                (wv_hbm, wv),
                (wq_hbm, wq),
                (wg_hbm, wg),
                (wo_hbm, wo),
                (in_gain_hbm, in_gain),
                (offset_hbm, offset),
                (head_gain_hbm, head_gain),
            )
        )
    ]
    loads[0].start()
    for one in loads[9:]:
        one.start()
    for one in loads[1:5]:
        one.start()

    barrier = pltpu.get_barrier_semaphore()

    def greet_sp(d, carry):
        pl.semaphore_signal(
            barrier, inc=1, device_id={"sp": lax.rem(me + d + 1, n)}, device_id_type=MESH
        )
        return carry

    loop(n - 1, greet_sp, 0)
    for d in range(1, n_tp):
        pl.semaphore_signal(
            barrier, inc=1, device_id={"tp": lax.rem(tp + d, n_tp)}, device_id_type=MESH
        )

    loads[0].wait()
    loads[5].start()
    loads[9].wait()
    step = 32

    def norm_rows(i, carry):
        where = pl.ds(pl.multiple_of(i * step, step), step)
        wide = tok[where, :].astype(F32)
        scale = lax.rsqrt(jnp.sum(wide * wide, axis=1, keepdims=True) * (1.0 / width) + EPS)
        nrm[where, :] = (wide * scale * in_gain[...]).astype(BF16)
        return carry

    lax.fori_loop(0, rows // step, norm_rows, 0, unroll=4)

    loads[1].wait()
    for one in loads[6:9]:
        one.start()
    k_s[...] = dot(nrm[...], wk[...]).astype(BF16)
    for i in (2, 3, 4, 10):
        loads[i].wait()
    low = dot_nt(nrm[...], down[...]).astype(BF16)
    logits = dot(low, up[...]) + offset[...]
    log_sig = jnp.minimum(logits, 0.0) - jnp.log1p(jnp.exp(-jnp.abs(logits)))
    extra[...] = log_sig * (1.0 / 16.0) + extra[...]
    tri = (
        lax.broadcasted_iota(jnp.int32, (BLK, BLK), 0)
        >= lax.broadcasted_iota(jnp.int32, (BLK, BLK), 1)
    )
    tri_ones = tri.astype(F32).astype(BF16)
    for b in range(blocks):
        hi, mid, lo = split3(extra[b * BLK:(b + 1) * BLK, :])
        cum_s[b * BLK:(b + 1) * BLK, :] = (
            dot(tri_ones, hi) + dot(tri_ones, mid) + dot(tri_ones, lo)
        )

    def span(h):
        return pl.ds(0, piece if h else piece + 16)

    def to_owner(h, p):
        return pltpu.make_async_remote_copy(
            src_ref=send1.at[h, p, span(h)], dst_ref=recv1.at[h, me, span(h)],
            send_sem=s1_sem.at[h, p], recv_sem=r1_sem.at[h, me],
            device_id={"sp": start + p}, device_id_type=MESH,
        )

    def from_source(h, i):
        return pltpu.make_async_remote_copy(
            src_ref=send1.at[h, 0, span(h)], dst_ref=recv1.at[h, i, span(h)],
            send_sem=s1_sem.at[h, 0], recv_sem=r1_sem.at[h, i],
            device_id={"sp": i}, device_id_type=MESH,
        )

    def to_user(h, i):
        return pltpu.make_async_remote_copy(
            src_ref=send2.at[h, i], dst_ref=recv2.at[h, own],
            send_sem=s2_sem.at[h, i], recv_sem=r2_sem.at[h, own],
            device_id={"sp": i}, device_id_type=MESH,
        )

    def from_owner(h, p):
        return pltpu.make_async_remote_copy(
            src_ref=send2.at[h, 0], dst_ref=recv2.at[h, p],
            send_sem=s2_sem.at[h, 0], recv_sem=r2_sem.at[h, p],
            device_id={"sp": start + p}, device_id_type=MESH,
        )

    totals = [cum_s[b * BLK + BLK - 1:(b + 1) * BLK, :] for b in range(blocks)]
    device_log = totals[0]
    for one in totals[1:]:
        device_log = device_log + one
    place = lax.broadcasted_iota(jnp.int32, (16, QF), 0)
    coded = jnp.zeros((16, QF), F32)
    for h in range(heads):
        for j, term in enumerate(split3(device_log[:, h * QF:(h + 1) * QF])):
            coded = jnp.where(place == 3 * h + j, term.astype(F32), coded)
    coded = coded.astype(BF16)

    loads[5].wait()
    for h in range(heads):
        ch = slice(h * QF, (h + 1) * QF)
        cols = slice(h * DV, (h + 1) * DV)
        v_s[:, cols] = dot(nrm[...], wv[:, cols]).astype(BF16)
        for b in range(blocks):
            part = slice(b * BLK, (b + 1) * BLK)
            total = totals[b][:, ch]
            closing = (k_s[part, ch].astype(F32) * jnp.exp(total - cum_s[part, ch])).astype(BF16)
            fresh = dot_tn(v_s[part, cols], closing)
            if b:
                fresh = fresh + before[b - 1, :, ch] * jnp.exp(total)
            before[b, :, ch] = fresh
        for p in range(owners):
            send1[h, p, :piece, :] = before[blocks - 1, p * piece:(p + 1) * piece, ch].astype(BF16)
            if h == 0:
                send1[h, p, piece:, :] = coded
        if h == 0:
            pl.semaphore_wait(barrier, n - 1 + n_tp - 1)

        @pl.when(me < n - 1)
        def _():
            def send_piece(d, carry):
                p = lax.rem(me + d, owners)

                @pl.when(start + p != me)
                def _():
                    to_owner(h, p).start()

                return carry

            loop(owners, send_piece, 0)

    loads[6].wait()
    for c in range(0, chans, 256):
        cols = slice(c, min(c + 256, chans))
        q_s[:, cols] = dot(nrm[...], wq[:, cols]).astype(BF16)

    device_log = jnp.zeros((1, chans), F32)
    for b in range(blocks):
        part = slice(b * BLK, (b + 1) * BLK)
        cum = cum_s[part, :]
        total = cum[BLK - 1:BLK, :]
        middle = cum[HALF - 1:HALF, :]
        query = q_s[part, :].astype(F32)
        key = k_s[part, :].astype(F32)
        query_inner = (query * jnp.exp(cum - middle)).astype(BF16)
        key_inner = (key * jnp.exp(middle - cum)).astype(BF16)
        qd_s[part, :] = (query * jnp.exp(cum + device_log)).astype(BF16)
        query_start = (query * jnp.exp(cum)).astype(BF16)
        for h in range(heads):
            ch = slice(h * QF, (h + 1) * QF)
            scores = dot_nt(query_inner[:, ch], key_inner[:, ch])
            scores = jnp.where(tri, scores, 0.0).astype(BF16)
            result = dot(scores, v_s[part, h * DV:(h + 1) * DV])
            if b:
                result = result + dot_nt(query_start[:, ch], before[b - 1, :, ch].astype(BF16))
            att[part, h * DV:(h + 1) * DV] = result
        device_log = device_log + total

    def prefixes(h):
        @pl.when(me < n - 1)
        def _():
            recv1[h, me, span(h)] = send1[h, own, span(h)]

        def one(i, state):
            rounded = state.astype(BF16)

            @pl.when(i == me)
            def _():
                recv2[h, own] = rounded

            @pl.when(jnp.logical_and(i != me, i > 0))
            def _():
                send2[h, i] = rounded
                to_user(h, i).start()

            @pl.when(jnp.logical_and(i != me, i < n - 1))
            def _():
                from_source(h, i).wait_recv()

            last = jnp.minimum(i, n - 2)
            tail = recv1[0, last, piece:piece + 16, :].astype(F32)
            t = 3 * h
            log = tail[t:t + 1, :] + tail[t + 1:t + 2, :] + tail[t + 2:t + 3, :]
            return state * jnp.exp(log) + recv1[h, last, :piece, :].astype(F32)

        loop(n, one, jnp.zeros((piece, QF), F32))

    @pl.when(owning)
    def _():
        for h in range(heads):
            prefixes(h)

    loads[7].wait()
    loads[11].wait()
    for c in range(vals // DV):
        cols = slice(c * DV, (c + 1) * DV)
        gate = dot(nrm[...], wg[:, cols]).astype(BF16).astype(F32)
        g_s[:, cols] = gate * jax.nn.sigmoid(gate) * head_gain[:, cols]

    def gather_copy(slot, h, b, to, which):
        part = pl.ds(b * BLK, BLK)
        return pltpu.make_async_remote_copy(
            src_ref=gath.at[slot, h, part], dst_ref=gath.at[slot, h, part],
            send_sem=gs_sem.at[which, h, b], recv_sem=gr_sem.at[which, h, b],
            device_id={"tp": to}, device_id_type=MESH,
        )

    def chip_at(d):
        return lax.rem(chip + d + chips, chips)

    @pl.when(me == 0)
    def _():
        recv2[...] = jnp.zeros_like(recv2)

    for h in range(heads):
        ch = slice(h * QF, (h + 1) * QF)
        cols = slice(h * DV, (h + 1) * DV)

        @pl.when(me > 0)
        def _():
            def take(p, carry):
                @pl.when(start + p != me)
                def _():
                    from_owner(h, p).wait_recv()

                return carry

            loop(owners, take, 0)

        carried = jnp.concatenate([recv2[h, p] for p in range(owners)], axis=0)
        for b in range(blocks):
            part = slice(b * BLK, (b + 1) * BLK)
            full = att[part, cols] + dot_nt(qd_s[part, ch], carried)
            scale = lax.rsqrt(jnp.mean(full * full, axis=1, keepdims=True) + EPS)
            gath[tp, h, part, :] = (full * scale * g_s[part, cols]).astype(BF16)
            for d in range(1, chips):
                gather_copy(tp, h, b, chip_at(d) * 2 + core, d).start()
            gather_copy(tp, h, b, partner, 0).start()

    loads[8].wait()

    def add(slot, h, part, begin):
        first = pl.multiple_of(slot * vals + h * DV, DV)
        value = dot(gath[slot, h, part, :], wo[pl.ds(first, DV), :])
        if begin:
            mix[part, :] = value
        else:
            mix[part, :] += value

    whole = slice(0, rows)
    for h in range(heads):
        add(tp, h, whole, h == 0)
    for h in range(heads):
        for b in range(blocks):
            gather_copy(partner, h, b, partner, 0).wait_recv()
        add(partner, h, whole, False)
    for h in range(heads):
        for d in range(1, chips):
            slot = chip_at(-d) * 2 + core
            for b in range(blocks):
                gather_copy(slot, h, b, partner, d).wait_recv()
                gather_copy(slot, h, b, partner, chips - 1 + d).start()
                if h == heads - 1:
                    add(slot, h, slice(b * BLK, (b + 1) * BLK), False)
            if h < heads - 1:
                add(slot, h, whole, False)
        for d in range(1, chips):
            slot = chip_at(-d) * 2 + (1 - core)
            if h < heads - 1:
                for b in range(blocks):
                    gather_copy(slot, h, b, partner, chips - 1 + d).wait_recv()
                add(slot, h, whole, False)
    def square_copy(d, b):
        return pltpu.make_async_remote_copy(
            src_ref=sq.at[0, b], dst_ref=sq.at[d, b],
            send_sem=qs_sem.at[d, b], recv_sem=qr_sem.at[d, b],
            device_id={"tp": lax.rem(tp + d, n_tp)}, device_id_type=MESH,
        )

    lanes = 128
    feats = wo.shape[1]
    for b in range(blocks):
        part = slice(b * BLK, (b + 1) * BLK)
        for d in range(1, chips):
            slot = chip_at(-d) * 2 + (1 - core)
            gather_copy(slot, heads - 1, b, partner, chips - 1 + d).wait_recv()
            add(slot, heads - 1, part, False)
        squares = jnp.zeros((BLK, lanes), F32)
        for c in range(0, feats, lanes):
            value = mix[part, c:c + lanes]
            squares = squares + value * value
        row = jnp.sum(squares.T, axis=0, keepdims=True)
        sq[0, b] = jnp.broadcast_to(row, (8, BLK))
        for d in range(1, n_tp):
            square_copy(d, b).start()

    for b in range(blocks):
        part = slice(b * BLK, (b + 1) * BLK)
        total = sq[0, b]
        for d in range(1, n_tp):
            square_copy(d, b).wait_recv()
            total = total + sq[d, b]
        row = jnp.broadcast_to(total[0:1, :], (lanes, BLK))
        scale = lax.rsqrt(row.T * (1.0 / width) + EPS)
        for c in range(0, feats, lanes):
            cols = slice(c, c + lanes)
            mix[part, cols] = mix[part, cols] * scale

    @pl.when(me < n - 1)
    def _():
        def drain(d, carry):
            p = lax.rem(me + d, owners)

            @pl.when(start + p != me)
            def _():
                for h in range(heads):
                    to_owner(h, p).wait_send()

            return carry

        loop(owners, drain, 0)

    @pl.when(owning)
    def _():
        def one(i, carry):
            @pl.when(jnp.logical_and(i != me, i > 0))
            def _():
                for h in range(heads):
                    to_user(h, i).wait_send()

            return carry

        loop(n, one, 0)

    for h in range(heads):
        for b in range(blocks):
            gather_copy(tp, h, b, partner, 0).wait_send()
            for d in range(1, chips):
                gather_copy(tp, h, b, partner, d).wait_send()
                gather_copy(tp, h, b, partner, chips - 1 + d).wait_send()
    for d in range(1, n_tp):
        for b in range(blocks):
            square_copy(d, b).wait_send()


def local(n, n_tp, *args):
    (tokens, in_gain, wq, wk, wv, wg, down, up, offset, extra, head_gain, wo, out_gain) = args
    rows, width = tokens.shape
    chans, vals, feats = wk.shape[1], wv.shape[1], wo.shape[1]
    blocks = rows // BLK
    piece = max(16, 2 * DV // n)
    owners = DV // piece
    start = (n - owners) // 2
    heads = chans // QF
    hbm = pl.BlockSpec(memory_space=pltpu.HBM)
    dma = pltpu.SemaphoreType.DMA
    scaled = pl.pallas_call(
        functools.partial(kernel, n, n_tp, owners, piece, start),
        out_shape=pltpu.VMEM((rows, feats), F32),
        in_specs=[hbm] * 12,
        out_specs=pl.BlockSpec(memory_space=pltpu.VMEM),
        scratch_shapes=[
            pltpu.VMEM(tokens.shape, BF16),
            pltpu.VMEM(wq.shape, BF16),
            pltpu.VMEM(wk.shape, BF16),
            pltpu.VMEM(wv.shape, BF16),
            pltpu.VMEM(wg.shape, BF16),
            pltpu.VMEM(down.shape[::-1], BF16),
            pltpu.VMEM((down.shape[1], chans), BF16),
            pltpu.VMEM(extra.shape, F32),
            pltpu.VMEM(wo.shape, BF16),
            pltpu.VMEM((1, width), F32),
            pltpu.VMEM((1, chans), F32),
            pltpu.VMEM((1, vals), F32),
            pltpu.VMEM((rows, width), BF16),
            pltpu.VMEM((rows, chans), BF16),
            pltpu.VMEM((rows, chans), BF16),
            pltpu.VMEM((rows, vals), BF16),
            pltpu.VMEM((rows, vals), F32),
            pltpu.VMEM((rows, chans), F32),
            pltpu.VMEM((rows, vals), F32),
            pltpu.VMEM((rows, chans), BF16),
            pltpu.VMEM((blocks, DV, chans), F32),
            pltpu.VMEM((heads, owners, piece + 16, QF), BF16),
            pltpu.VMEM((heads, n, piece + 16, QF), BF16),
            pltpu.VMEM((heads, n, piece, QF), BF16),
            pltpu.VMEM((heads, owners, piece, QF), BF16),
            pltpu.VMEM((n_tp, heads, rows, DV), BF16),
            pltpu.VMEM((n_tp, blocks, 8, BLK), F32),
            dma((12,)),
            dma((heads, owners)),
            dma((heads, n)),
            dma((heads, n)),
            dma((heads, owners)),
            dma((n_tp, heads, blocks)),
            dma((n_tp, heads, blocks)),
            dma((n_tp, blocks)),
            dma((n_tp, blocks)),
        ],
        compiler_params=pltpu.CompilerParams(
            collective_id=0, has_side_effects=True, vmem_limit_bytes=66000000
        ),
    )(
        tokens, in_gain[None], wq, wk, wv, wg, down.T, up, offset[None], extra,
        head_gain[None], wo,
    )
    return (scaled * out_gain[None]).astype(BF16)


def solution(mesh):
    placed = (
        P("sp", None),
        P(),
        P(None, "tp"),
        P(None, "tp"),
        P(None, "tp"),
        P(None, "tp"),
        P(),
        P(),
        P("tp"),
        P("sp", "tp"),
        P("tp"),
        P(None, "tp"),
        P("tp"),
    )
    return jax.shard_map(
        functools.partial(local, mesh.shape["sp"], mesh.shape["tp"]),
        mesh=mesh, in_specs=placed, out_specs=P("sp", "tp"), check_vma=False,
    )
```

profile of v0, /device:TPU:10, one launch (start us, length us, event | category | flops | bytes accessed | tf_op | source)
XLA Modules:
  0.0 28.7 jit_solution(7112081732352761425)
XLA Ops:
  0.0 0.0 copy-start
  0.0 27.8 %shard_map.127 = f32[384,512]{1,0:T(8,128)S(1)} custom-call(bf16[384,2048]{1,0:T(8,128)(2,1)} %tok_hbm.1, f32[1,2048]{1,0:T(1,128)} %bitcast.5, bf16[2048,256]{1,0:T(8,128)(2,1)} %wq_hbm.1, bf16[2048,256]{1,0:T(8,128)(2,1)} %wk_hbm.1, bf16[2048,512]{1,0:T(8,128)(2,1)} %wv_hbm.1, bf16[2048,512]{1,0:T(8,128)(2,1)} %wg_hbm.1, bf16[32,2048]{1,0:T(8,128)(2,1)} %bitcast.4, ...), custom_call_target="tpu_custom_call" | custom-call | tf_op jit(solution)/shard_map/pallas_call | solution.py:447
  27.8 0.0 copy-done
  27.8 0.8 %multiply_convert_fusion = bf16[384,512]{1,0:T(8,128)(2,1)} fusion(f32[384,512]{1,0:T(8,128)S(1)} %shard_map.127, f32[512]{0:T(512)S(1)} %copy-done), kind=kLoop, calls=%fused_computation | loop fusion | flops 393216 | bytes 1181696 | tf_op jit(solution)/shard_map/convert_element_type | solution.py:497
Async XLA Ops:
  0.0 27.8 %copy-start = (f32[512]{0:T(512)S(1)}, f32[512]{0:T(512)}, u32[]{:S(2)}) copy-start(f32[512]{0:T(512)} %param.25) | copy-start | bytes 6148
where the time goes:
time: 29.1 us; the launch traced here: 28.7 us
  Pallas kernels  27.8 us (96%)
  other arithmetic  0.83 us (3%)
    pallas_call x1, Pallas kernels, local(): pl.pallas_call(functools.partial(kernel, n, n_tp, owners, piece, start),...  27.8 us
    convert_element_type x1, other arithmetic, local(): return (scaled * out_gain[None]).astype(BF16)  0.83 us

commit v1 on v0

v1 whole, which is shorter than its diff:
```python
import functools

import jax
import jax.numpy as jnp
from jax import lax
from jax.experimental import pallas as pl
from jax.experimental.pallas import tpu as pltpu
from jax.sharding import PartitionSpec as P

QF = 128
DV = 256
BLK = 128
HALF = 64
TOK_CHUNKS = 4
EPS = 1e-06
F32 = jnp.float32
BF16 = jnp.bfloat16
MESH = pl.DeviceIdType.MESH


def loop(count, body, carry):
    if count <= 16:
        for i in range(count):
            carry = body(i, carry)
        return carry
    return lax.fori_loop(0, count, body, carry)


def split3(x):
    hi = x.astype(BF16)
    rest = x - hi.astype(F32)
    mid = rest.astype(BF16)
    lo = (rest - mid.astype(F32)).astype(BF16)
    return hi, mid, lo


def dot(a, b):
    return jnp.dot(a, b, preferred_element_type=F32)


def dot_nt(a, b):
    return lax.dot_general(a, b, (((1,), (1,)), ((), ())), preferred_element_type=F32)


def dot_tn(a, b):
    return lax.dot_general(a, b, (((0,), (0,)), ((), ())), preferred_element_type=F32)


def kernel(
    n, n_tp, owners, piece, start,
    tok_hbm, in_gain_hbm, wq_hbm, wk_hbm, wv_hbm, wg_hbm, down_hbm, up_hbm, offset_hbm,
    extra_hbm, head_gain_hbm, wo_hbm, out_gain_hbm,
    out,
    tok, wq, wk, wv, wg, down, up, extra, wo, in_gain, offset, head_gain, out_gain,
    nrm, q_s, k_s, v_s, g_s, cum_s, att, qd_s, before, mix,
    send1, recv1, send2, recv2, logs, gath, sq,
    tok_sem, load_sem, sl_sem, rl_sem, s1_sem, r1_sem, s2_sem, r2_sem,
    gs_sem, gr_sem, qs_sem, qr_sem,
):
    rows, width = tok.shape
    chans = wk.shape[1]
    heads = chans // QF
    vals = wv.shape[1]
    blocks = rows // BLK
    me = lax.axis_index("sp")
    tp = lax.axis_index("tp")
    chips = n_tp // 2
    core = lax.rem(tp, 2)
    chip = tp // 2
    partner = chip * 2 + (1 - core)
    own = me - start
    owning = jnp.logical_and(own >= 0, own < owners)

    first = pl.multiple_of(tp * chans, chans)
    chunk = rows // TOK_CHUNKS
    tok_load = [
        pltpu.make_async_copy(
            tok_hbm.at[pl.ds(i * chunk, chunk)], tok.at[pl.ds(i * chunk, chunk)], tok_sem.at[i]
        )
        for i in range(TOK_CHUNKS)
    ]
    load = {
        name: pltpu.make_async_copy(src, dst, load_sem.at[i])
        for i, (name, src, dst) in enumerate(
            (
                ("in_gain", in_gain_hbm, in_gain),
                ("wk", wk_hbm, wk),
                ("down", down_hbm, down),
                ("up", up_hbm.at[:, pl.ds(first, chans)], up),
                ("extra", extra_hbm, extra),
                ("offset", offset_hbm, offset),
                ("wv", wv_hbm, wv),
                ("wq", wq_hbm, wq),
                ("wg", wg_hbm, wg),
                ("head_gain", head_gain_hbm, head_gain),
                ("wo", wo_hbm, wo),
                ("out_gain", out_gain_hbm, out_gain),
            )
        )
    }

    def begin(*names):
        for name in names:
            load[name].start()

    def arrive(*names):
        for name in names:
            load[name].wait()

    begin("in_gain")
    for one in tok_load:
        one.start()
    begin("down", "wk", "up", "offset", "extra")

    barrier = pltpu.get_barrier_semaphore()

    def greet_sp(d, carry):
        pl.semaphore_signal(
            barrier, inc=1, device_id={"sp": lax.rem(me + d + 1, n)}, device_id_type=MESH
        )
        return carry

    loop(n - 1, greet_sp, 0)
    for d in range(1, n_tp):
        pl.semaphore_signal(
            barrier, inc=1, device_id={"tp": lax.rem(tp + d, n_tp)}, device_id_type=MESH
        )

    step = 32
    arrive("in_gain")
    for i in range(TOK_CHUNKS):
        tok_load[i].wait()
        if i == TOK_CHUNKS - 2:
            begin("wv")

        def norm_rows(j, carry):
            where = pl.ds(pl.multiple_of(i * chunk + j * step, step), step)
            wide = tok[where, :].astype(F32)
            scale = lax.rsqrt(jnp.sum(wide * wide, axis=1, keepdims=True) * (1.0 / width) + EPS)
            nrm[where, :] = (wide * scale * in_gain[...]).astype(BF16)
            return carry

        lax.fori_loop(0, chunk // step, norm_rows, 0, unroll=True)

    arrive("down", "wk")
    begin("wq", "wg", "head_gain", "wo", "out_gain")
    low = dot_nt(nrm[...], down[...]).astype(BF16)
    k_s[...] = dot(nrm[...], wk[...]).astype(BF16)
    arrive("up", "offset", "extra", "wv")
    logits = dot(low, up[...]) + offset[...]
    log_sig = jnp.minimum(logits, 0.0) - jnp.log1p(jnp.exp(-jnp.abs(logits)))
    decay = log_sig * (1.0 / 16.0) + extra[...]
    tri = (
        lax.broadcasted_iota(jnp.int32, (BLK, BLK), 0)
        >= lax.broadcasted_iota(jnp.int32, (BLK, BLK), 1)
    )
    tri_ones = tri.astype(F32).astype(BF16)
    for h in range(heads):
        cols = slice(h * DV, (h + 1) * DV)
        v_s[:, cols] = dot(nrm[...], wv[:, cols]).astype(BF16)
    for b in range(blocks):
        hi, mid, lo = split3(decay[b * BLK:(b + 1) * BLK, :])
        cum_s[b * BLK:(b + 1) * BLK, :] = (
            dot(tri_ones, hi) + dot(tri_ones, mid) + dot(tri_ones, lo)
        )
    totals = [cum_s[b * BLK + BLK - 1:(b + 1) * BLK, :] for b in range(blocks)]
    device_log = totals[0]
    for one in totals[1:]:
        device_log = device_log + one
    logs[me] = device_log

    def log_to_owner(p):
        return pltpu.make_async_remote_copy(
            src_ref=logs.at[me], dst_ref=logs.at[me], send_sem=sl_sem, recv_sem=rl_sem,
            device_id={"sp": start + p}, device_id_type=MESH,
        )

    def to_owner(h, p):
        return pltpu.make_async_remote_copy(
            src_ref=send1.at[h, p], dst_ref=recv1.at[h, me],
            send_sem=s1_sem, recv_sem=r1_sem.at[h, me],
            device_id={"sp": start + p}, device_id_type=MESH,
        )

    def from_source(h, i):
        return pltpu.make_async_remote_copy(
            src_ref=send1.at[h, 0], dst_ref=recv1.at[h, i],
            send_sem=s1_sem, recv_sem=r1_sem.at[h, i],
            device_id={"sp": i}, device_id_type=MESH,
        )

    def to_user(h, i):
        return pltpu.make_async_remote_copy(
            src_ref=send2.at[h, i], dst_ref=recv2.at[h, own],
            send_sem=s2_sem, recv_sem=r2_sem.at[h],
            device_id={"sp": i}, device_id_type=MESH,
        )

    def settle(ref, sem):
        pltpu.make_async_copy(ref, ref, sem).wait()

    def each_owner(action):
        @pl.when(me < n - 1)
        def _():
            def one(d, carry):
                p = lax.rem(me + d, owners)

                @pl.when(start + p != me)
                def _():
                    action(p)

                return carry

            loop(owners, one, 0)

    pl.semaphore_wait(barrier, n - 1 + n_tp - 1)
    each_owner(lambda p: log_to_owner(p).start())

    for h in range(heads):
        ch = slice(h * QF, (h + 1) * QF)
        cols = slice(h * DV, (h + 1) * DV)
        for b in range(blocks):
            part = slice(b * BLK, (b + 1) * BLK)
            total = totals[b][:, ch]
            closing = (k_s[part, ch].astype(F32) * jnp.exp(total - cum_s[part, ch])).astype(BF16)
            fresh = dot_tn(v_s[part, cols], closing)
            if b:
                fresh = fresh + before[b - 1, :, ch] * jnp.exp(total)
            before[b, :, ch] = fresh
        for p in range(owners):
            send1[h, p] = before[blocks - 1, p * piece:(p + 1) * piece, ch].astype(BF16)
        each_owner(lambda p: to_owner(h, p).start())

    arrive("wq", "wg", "head_gain")
    for c in range(0, chans, 256):
        cols = slice(c, min(c + 256, chans))
        q_s[:, cols] = dot(nrm[...], wq[:, cols]).astype(BF16)
    for c in range(vals // DV):
        cols = slice(c * DV, (c + 1) * DV)
        gate = dot(nrm[...], wg[:, cols]).astype(BF16).astype(F32)
        g_s[:, cols] = gate * jax.nn.sigmoid(gate) * head_gain[:, cols]

    device_log = jnp.zeros((1, chans), F32)
    for b in range(blocks):
        part = slice(b * BLK, (b + 1) * BLK)
        cum = cum_s[part, :]
        total = cum[BLK - 1:BLK, :]
        middle = cum[HALF - 1:HALF, :]
        query = q_s[part, :].astype(F32)
        key = k_s[part, :].astype(F32)
        query_inner = (query * jnp.exp(cum - middle)).astype(BF16)
        key_inner = (key * jnp.exp(middle - cum)).astype(BF16)
        qd_s[part, :] = (query * jnp.exp(cum + device_log)).astype(BF16)
        query_start = (query * jnp.exp(cum)).astype(BF16)
        for h in range(heads):
            ch = slice(h * QF, (h + 1) * QF)
            scores = dot_nt(query_inner[:, ch], key_inner[:, ch])
            scores = jnp.where(tri, scores, 0.0).astype(BF16)
            result = dot(scores, v_s[part, h * DV:(h + 1) * DV])
            if b:
                result = result + dot_nt(query_start[:, ch], before[b - 1, :, ch].astype(BF16))
            att[part, h * DV:(h + 1) * DV] = result
        device_log = device_log + total

    def prefixes(h):
        recv1[h, me] = send1[h, own]

        def one(i, state):
            rounded = state.astype(BF16)

            @pl.when(i == me)
            def _():
                recv2[h, own] = rounded

            @pl.when(jnp.logical_and(i != me, i > 0))
            def _():
                send2[h, i] = rounded
                to_user(h, i).start()

            @pl.when(jnp.logical_and(i != me, i < n - 1))
            def _():
                from_source(h, i).wait_recv()

            last = jnp.minimum(i, n - 2)
            log = logs[last][:, h * QF:(h + 1) * QF]
            return state * jnp.exp(log) + recv1[h, last].astype(F32)

        loop(n, one, jnp.zeros((piece, QF), F32))

    @pl.when(owning)
    def _():
        settle(logs.at[pl.ds(0, n - 2)], rl_sem)
        for h in range(heads):
            prefixes(h)

    def gather_copy(slot, h, b, to, which):
        part = pl.ds(b * BLK, BLK)
        return pltpu.make_async_remote_copy(
            src_ref=gath.at[slot, h, part], dst_ref=gath.at[slot, h, part],
            send_sem=gs_sem, recv_sem=gr_sem.at[which, h, b],
            device_id={"tp": to}, device_id_type=MESH,
        )

    def chip_at(d):
        return lax.rem(chip + d + chips, chips)

    @pl.when(me == 0)
    def _():
        recv2[...] = jnp.zeros_like(recv2)

    for h in range(heads):
        ch = slice(h * QF, (h + 1) * QF)
        cols = slice(h * DV, (h + 1) * DV)

        @pl.when(owning)
        def _():
            settle(recv2.at[h, pl.ds(0, owners - 1)], r2_sem.at[h])

        @pl.when(jnp.logical_and(me > 0, jnp.logical_not(owning)))
        def _():
            settle(recv2.at[h], r2_sem.at[h])

        carried = jnp.concatenate([recv2[h, p] for p in range(owners)], axis=0)
        for b in range(blocks):
            part = slice(b * BLK, (b + 1) * BLK)
            full = att[part, cols] + dot_nt(qd_s[part, ch], carried)
            scale = lax.rsqrt(jnp.mean(full * full, axis=1, keepdims=True) + EPS)
            gath[tp, h, part, :] = (full * scale * g_s[part, cols]).astype(BF16)
            for d in range(1, chips):
                gather_copy(tp, h, b, chip_at(d) * 2 + core, d).start()
            gather_copy(tp, h, b, partner, 0).start()

    arrive("wo", "out_gain")

    def add(slot, h, part, begin):
        first = pl.multiple_of(slot * vals + h * DV, DV)
        value = dot(gath[slot, h, part, :], wo[pl.ds(first, DV), :])
        if begin:
            mix[part, :] = value
        else:
            mix[part, :] += value

    whole = slice(0, rows)
    for h in range(heads):
        add(tp, h, whole, h == 0)
    for h in range(heads):
        for b in range(blocks):
            gather_copy(partner, h, b, partner, 0).wait_recv()
        add(partner, h, whole, False)
    for h in range(heads):
        for d in range(1, chips):
            slot = chip_at(-d) * 2 + core
            for b in range(blocks):
                gather_copy(slot, h, b, partner, d).wait_recv()
                gather_copy(slot, h, b, partner, chips - 1 + d).start()
                if h == heads - 1:
                    add(slot, h, slice(b * BLK, (b + 1) * BLK), False)
            if h < heads - 1:
                add(slot, h, whole, False)
        for d in range(1, chips):
            slot = chip_at(-d) * 2 + (1 - core)
            if h < heads - 1:
                for b in range(blocks):
                    gather_copy(slot, h, b, partner, chips - 1 + d).wait_recv()
                add(slot, h, whole, False)
    def square_copy(d, b):
        return pltpu.make_async_remote_copy(
            src_ref=sq.at[0, b], dst_ref=sq.at[d, b],
            send_sem=qs_sem, recv_sem=qr_sem.at[b],
            device_id={"tp": lax.rem(tp + d, n_tp)}, device_id_type=MESH,
        )

    lanes = 128
    feats = wo.shape[1]
    for b in range(blocks):
        part = slice(b * BLK, (b + 1) * BLK)
        for d in range(1, chips):
            slot = chip_at(-d) * 2 + (1 - core)
            gather_copy(slot, heads - 1, b, partner, chips - 1 + d).wait_recv()
            add(slot, heads - 1, part, False)
        squares = jnp.zeros((BLK, lanes), F32)
        for c in range(0, feats, lanes):
            value = mix[part, c:c + lanes]
            squares = squares + value * value
        row = jnp.sum(squares.T, axis=0, keepdims=True)
        sq[0, b] = jnp.broadcast_to(row, (8, BLK))
        for d in range(1, n_tp):
            square_copy(d, b).start()

    for b in range(blocks):
        part = slice(b * BLK, (b + 1) * BLK)
        settle(sq.at[pl.ds(1, n_tp - 1), b], qr_sem.at[b])
        total = sq[0, b]
        for d in range(1, n_tp):
            total = total + sq[d, b]
        row = jnp.broadcast_to(total[0:1, :], (lanes, BLK))
        scale = lax.rsqrt(row.T * (1.0 / width) + EPS)
        for c in range(0, feats, lanes):
            cols = slice(c, c + lanes)
            out[part, cols] = (mix[part, cols] * scale * out_gain[:, cols]).astype(BF16)

    @pl.when(owning)
    def _():
        settle(logs.at[pl.ds(0, owners - 1)], sl_sem)
        settle(send1.at[:, pl.ds(0, owners - 1)], s1_sem)
        settle(send2.at[:, pl.ds(0, n - 2)], s2_sem)

    @pl.when(jnp.logical_and(me < n - 1, jnp.logical_not(owning)))
    def _():
        settle(logs.at[pl.ds(0, owners)], sl_sem)
        settle(send1, s1_sem)

    settle(gath.at[pl.ds(0, n_tp - 1)], gs_sem)
    settle(sq.at[pl.ds(1, n_tp - 1)], qs_sem)


def local(n, n_tp, *args):
    (tokens, in_gain, wq, wk, wv, wg, down, up, offset, extra, head_gain, wo, out_gain) = args
    rows, width = tokens.shape
    chans, vals, feats = wk.shape[1], wv.shape[1], wo.shape[1]
    blocks = rows // BLK
    piece = max(16, 2 * DV // n)
    owners = DV // piece
    start = (n - owners) // 2
    heads = chans // QF
    hbm = pl.BlockSpec(memory_space=pltpu.HBM)
    dma = pltpu.SemaphoreType.DMA
    return pl.pallas_call(
        functools.partial(kernel, n, n_tp, owners, piece, start),
        out_shape=pltpu.VMEM((rows, feats), BF16),
        in_specs=[hbm] * 13,
        out_specs=pl.BlockSpec(memory_space=pltpu.VMEM),
        scratch_shapes=[
            pltpu.VMEM(tokens.shape, BF16),
            pltpu.VMEM(wq.shape, BF16),
            pltpu.VMEM(wk.shape, BF16),
            pltpu.VMEM(wv.shape, BF16),
            pltpu.VMEM(wg.shape, BF16),
            pltpu.VMEM(down.shape[::-1], BF16),
            pltpu.VMEM((down.shape[1], chans), BF16),
            pltpu.VMEM(extra.shape, F32),
            pltpu.VMEM(wo.shape, BF16),
            pltpu.VMEM((1, width), F32),
            pltpu.VMEM((1, chans), F32),
            pltpu.VMEM((1, vals), F32),
            pltpu.VMEM((1, feats), F32),
            pltpu.VMEM((rows, width), BF16),
            pltpu.VMEM((rows, chans), BF16),
            pltpu.VMEM((rows, chans), BF16),
            pltpu.VMEM((rows, vals), BF16),
            pltpu.VMEM((rows, vals), F32),
            pltpu.VMEM((rows, chans), F32),
            pltpu.VMEM((rows, vals), F32),
            pltpu.VMEM((rows, chans), BF16),
            pltpu.VMEM((blocks, DV, chans), F32),
            pltpu.VMEM((rows, feats), F32),
            pltpu.VMEM((heads, owners, piece, QF), BF16),
            pltpu.VMEM((heads, n, piece, QF), BF16),
            pltpu.VMEM((heads, n, piece, QF), BF16),
            pltpu.VMEM((heads, owners, piece, QF), BF16),
            pltpu.VMEM((n, 1, chans), F32),
            pltpu.VMEM((n_tp, heads, rows, DV), BF16),
            pltpu.VMEM((n_tp, blocks, 8, BLK), F32),
            dma((TOK_CHUNKS,)),
            dma((12,)),
            dma,
            dma,
            dma,
            dma((heads, n)),
            dma,
            dma((heads,)),
            dma,
            dma((n_tp - 1, heads, blocks)),
            dma,
            dma((blocks,)),
        ],
        compiler_params=pltpu.CompilerParams(
            collective_id=0, has_side_effects=True, vmem_limit_bytes=66000000
        ),
    )(
        tokens, in_gain[None], wq, wk, wv, wg, down.T, up, offset[None], extra,
        head_gain[None], wo, out_gain[None],
    )


def solution(mesh):
    placed = (
        P("sp", None),
        P(),
        P(None, "tp"),
        P(None, "tp"),
        P(None, "tp"),
        P(None, "tp"),
        P(),
        P(),
        P("tp"),
        P("sp", "tp"),
        P("tp"),
        P(None, "tp"),
        P("tp"),
    )
    return jax.shard_map(
        functools.partial(local, mesh.shape["sp"], mesh.shape["tp"]),
        mesh=mesh, in_specs=placed, out_specs=P("sp", "tp"), check_vma=False,
    )
```

time: 29.1 us -> 27.1 us (0.931)
  the two profiles are of different devices: /device:TPU:10 before, /device:TPU:15 now
where the time goes in v1:
time: 27.1 us; the launch traced here: 26.9 us
  Pallas kernels  26.1 us (96%)
  local copies, waits for them, and re-layouts  0.75 us (3%)
    pallas_call x1, Pallas kernels, local(): pl.pallas_call(functools.partial(kernel, n, n_tp, owners, piece, start),...  26.1 us
    unnamed x1, local copies, waits for them, and re-layouts  0.75 us

profile of v1, /device:TPU:15, one launch (start us, length us, event | category | flops | bytes accessed | tf_op | source)
XLA Modules:
  0.0 26.9 jit_solution(16476771430092215253)
XLA Ops:
  0.0 26.1 %shard_map.127 = bf16[384,512]{1,0:T(8,128)(2,1)S(1)} custom-call(bf16[384,2048]{1,0:T(8,128)(2,1)} %tok_hbm.1, f32[1,2048]{1,0:T(1,128)} %bitcast.6, bf16[2048,256]{1,0:T(8,128)(2,1)} %wq_hbm.1, bf16[2048,256]{1,0:T(8,128)(2,1)} %wk_hbm.1, bf16[2048,512]{1,0:T(8,128)(2,1)} %wv_hbm.1, bf16[2048,512]{1,0:T(8,128)(2,1)} %wg_hbm.1, bf16[32,2048]{1,0:T(8,128)(2,1)} %bitcast.5, ...), custom_call_target="tpu_custom_call" | custom-call | tf_op jit(solution)/shard_map/pallas_call | solution.py:428
  26.2 0.7 %copy.15 = bf16[384,512]{1,0:T(8,128)(2,1)} copy(bf16[384,512]{1,0:T(8,128)(2,1)S(1)} %shard_map.127) | data formatting | bytes 786432
